TPU v7x, 32 devices: a whole 2x2x4 slice. The times are simulated.
32 devices in a mesh: sp: 8 (over z, y), tp: 4 (over x, core).
Axes of the slice: x: 2, y: 2, z: 4, core: 2. Of those that a mesh axis runs over, the one named last changes fastest.
Arguments:
- stream: bfloat16 [4096, 2048], P('sp', 'tp'), may hold values from -6 to 6
- doc_ids: int32 [4096], P('sp'), may hold values from 0 to 3, never falling along the last dimension, each value on 1 to 2304 neighbouring positions
- norm_gain: float32 [2, 2048], replicated, may hold values from 0.1 to 1.9
- gate_proj: bfloat16 [2, 2048, 2048], P(None, 'sp', 'tp'), may hold values from -0.125 to 0.125
- input_gate: bfloat16 [2, 2048, 2048], P(None, 'sp', 'tp'), may hold values from -0.125 to 0.125
- value_proj: bfloat16 [2, 2048, 2048], P(None, 'sp', 'tp'), may hold values from -0.125 to 0.125
- taps: float32 [2, 3, 2048], P(None, None, 'tp'), may hold values from -3 to 3
- out_proj: bfloat16 [2, 2048, 2048], P(None, 'tp', 'sp'), may hold values from -0.125 to 0.125
Outputs:
- result: bfloat16 [4096, 2048], P('sp', 'tp')
Inputs may be any that keep to these rules, and one draw needn't show every extreme that they name: `doc_ids`: document numbers never fall along the sequence; each document holds 1 to 2304 positions.
All inputs are finite; a program needn't handle non-finite values.
Results may differ from a plain program's by a relative error of at most 0.03.
Values may be sent and summed in bfloat16 or wider, within the bound.
A program may use at most 64 MiB of HBM per device.

v0:
```python
import jax
import jax.numpy as jnp
from jax import lax
from jax.sharding import PartitionSpec as P

epsilon = 1e-06


def with_halo(value, sides, width):
    for axis, dim in sides:
        size, length = (lax.axis_size(axis), value.shape[dim])
        up = [(i, (i + 1) % size) for i in range(size - 1)]
        down = [(j, i) for i, j in up]
        last = lax.slice_in_dim(value, length - width, length, axis=dim)
        leading = lax.slice_in_dim(value, 0, width, axis=dim)
        before = lax.ppermute(last, axis, up)
        after = lax.ppermute(leading, axis, down)
        value = jnp.concatenate([before, value, after], axis=dim)
    return value


def per_device(stream, doc_ids, norm_gain, gate_proj, input_gate, value_proj, taps, out_proj):
    layers = gate_proj.shape[0]
    gathered_in = (
        lax.all_gather(gate_proj, "sp", axis=1, tiled=True),
        lax.all_gather(input_gate, "sp", axis=1, tiled=True),
        lax.all_gather(value_proj, "sp", axis=1, tiled=True),
    )
    gathered_out = lax.all_gather(out_proj, "sp", axis=2, tiled=True)
    current = stream
    for layer_index in range(layers):
        full_rows = lax.all_gather(current, "tp", axis=1, tiled=True)
        widened = full_rows.astype(jnp.float32)
        scale = lax.rsqrt(jnp.mean(widened * widened, axis=-1, keepdims=True) + epsilon)
        normed = (widened * scale * norm_gain[layer_index]).astype(jnp.bfloat16)
        gate_b = jnp.dot(normed, gathered_in[0][layer_index], preferred_element_type=jnp.float32)
        gate_c = jnp.dot(normed, gathered_in[1][layer_index], preferred_element_type=jnp.float32)
        values = jnp.dot(normed, gathered_in[2][layer_index], preferred_element_type=jnp.float32)
        gate_b = gate_b.astype(jnp.bfloat16)
        gate_c = gate_c.astype(jnp.bfloat16)
        values = values.astype(jnp.bfloat16)
        mixed_in = (gate_c.astype(jnp.float32) * values.astype(jnp.float32)).astype(jnp.bfloat16)
        padded, doc_padded = (
            with_halo(mixed_in, (("sp", 0),), 1),
            with_halo(doc_ids, (("sp", 0),), 1),
        )
        same_prev = (doc_padded[:-2] == doc_ids)[:, None]
        same_next = (doc_padded[2:] == doc_ids)[:, None]
        kernel_taps = taps[layer_index]
        convolved = (
            jnp.where(same_prev, kernel_taps[0] * padded[:-2].astype(jnp.float32), 0.0)
            + kernel_taps[1] * mixed_in.astype(jnp.float32)
            + jnp.where(same_next, kernel_taps[2] * padded[2:].astype(jnp.float32), 0.0)
        )
        gated = (gate_b.astype(jnp.float32) * convolved).astype(jnp.bfloat16)
        partials = jnp.dot(gated, gathered_out[layer_index], preferred_element_type=jnp.float32)
        summed = lax.psum_scatter(
            partials.astype(jnp.bfloat16), "tp", scatter_dimension=1, tiled=True
        ).astype(jnp.float32)
        current = (current.astype(jnp.float32) + summed).astype(jnp.bfloat16)
    return current


def solution(mesh):
    in_specs = (
        P("sp", "tp"),
        P("sp"),
        P(),
        P(None, "sp", "tp"),
        P(None, "sp", "tp"),
        P(None, "sp", "tp"),
        P(None, None, "tp"),
        P(None, "tp", "sp"),
    )
    out_specs = P("sp", "tp")
    return jax.shard_map(
        per_device, mesh=mesh, in_specs=in_specs, out_specs=out_specs, check_vma=False
    )
```

profile of v0, /device:TPU:0, one launch (start us, length us, event | category | flops | bytes accessed | tf_op | source)
XLA Modules:
  0.0 454.6 jit_solution(15519410524372381653)
XLA Ops:
  6.5 0.7 all-gather.7.cloned.1.call-update
  7.3 0.0 all-gather.13.cloned.1.call-start
  7.3 0.7 all-gather.13.cloned.1.call-update
  8.0 0.0 all-gather.11.cloned.1.call-start
  8.1 0.7 all-gather.11.cloned.1.call-update
  8.7 0.0 all-gather.9.cloned.1.call-start
  8.8 0.5 all-gather.9.cloned.1.call-update
  9.3 0.0 all-gather.15.cloned.1.call-start
  9.4 0.5 all-gather.15.cloned.1.call-update
  9.9 0.0 reduce-scatter.3.cloned.1.call-start
  9.9 1.3 fusion.64
  11.3 5.4 %collective-permute-start = (s32[1]{0:T(128)}, s32[1]{0:T(128)}, u32[]{:S(2)}, u32[]{:S(2)}) collective-permute-start(s32[1]{0:T(128)} %get-tuple-element.21), channel_id=1, source_target_pairs={{0,4},{4,8},{8,12},{12,16},{16,20},{20,24},{24,28},{1,5},{5,9},{9,... | collective-permute-start | bytes 20 | tf_op jit(solution)/shard_map/ppermute | solution.py:16
  16.7 1.3 collective-permute-start.2
  18.0 0.8 fusion.63
  18.8 0.8 fusion.62
  19.6 2.5 collective-permute-done.2
  22.2 2.1 pad_add_fusion
  24.3 9.9 %all-gather.7.cloned.1.call-done = bf16[512,2048]{1,0:T(8,128)(2,1)} async-done(((bf16[512,512]{1,0:T(8,128)(2,1)}), bf16[512,2048]{1,0:T(8,128)(2,1)}) %all-gather.7.cloned.1.call-update) | async-done | bytes 2097168 | tf_op jit(solution)/shard_map/all_gather | solution.py:32
  34.2 2.1 fusion
  36.3 72.9 %all-gather.13.cloned.1.call-done = bf16[2,2048,512]{2,1,0:T(8,128)(2,1)} async-done(((bf16[2,256,512]{2,1,0:T(8,128)(2,1)}), bf16[2,2048,512]{2,1,0:T(8,128)(2,1)}) %all-gather.13.cloned.1.call-update) | async-done | bytes 4194320 | tf_op jit(solution)/shard_map/all_gather | solution.py:27
  109.2 4.7 %fusion.19 = f32[512,512]{1,0:T(8,128)} fusion(bf16[2,2048,512]{2,1,0:T(8,128)(2,1)} %all-gather.13.cloned.1.call-done, bf16[512,2048]{1,0:T(8,128)(2,1)} %all-gather.7.cloned.1.call-done, f32[2048]{0:T(1024)S(1)} %bitcast.79, f32[512]{0:T(512)S(1)} %add_rsqrt_fusion.1), kind=kOutput, calls=%fused_computation.33 | convolution fusion | flops 1078460416 | bytes 5253120 | tf_op jit(solution)/shard_map/dot_general | solution.py:38
  113.9 68.9 %all-gather.11.cloned.1.call-done = bf16[2,2048,512]{2,1,0:T(8,128)(2,1)} async-done(((bf16[2,256,512]{2,1,0:T(8,128)(2,1)}), bf16[2,2048,512]{2,1,0:T(8,128)(2,1)}) %all-gather.11.cloned.1.call-update) | async-done | bytes 4194320 | tf_op jit(solution)/shard_map/all_gather | solution.py:26
  182.7 3.1 fusion.30
  185.9 2.5 collective-permute-start.1
  188.4 1.3 collective-permute-start.3
  189.7 0.1 slice_compare_fusion.1
  189.8 66.4 %all-gather.9.cloned.1.call-done = bf16[2,2048,512]{2,1,0:T(8,128)(2,1)} async-done(((bf16[2,256,512]{2,1,0:T(8,128)(2,1)}), bf16[2,2048,512]{2,1,0:T(8,128)(2,1)}) %all-gather.9.cloned.1.call-update) | async-done | bytes 4194320 | tf_op jit(solution)/shard_map/all_gather | solution.py:25
  256.1 75.1 %all-gather.15.cloned.1.call-done = bf16[2,512,2048]{2,1,0:T(8,128)(2,1)} async-done(((bf16[2,512,256]{2,1,0:T(8,128)(2,1)}), bf16[2,512,2048]{2,1,0:T(8,128)(2,1)}) %all-gather.15.cloned.1.call-update) | async-done | bytes 4194320 | tf_op jit(solution)/shard_map/all_gather | solution.py:29
  331.2 6.3 %convolution_convert_fusion.1 = bf16[512,2048]{1,0:T(8,128)(2,1)} fusion(bf16[2,512,2048]{2,1,0:T(8,128)(2,1)} %all-gather.15.cloned.1.call-done, bf16[2,2048,512]{2,1,0:T(8,128)(2,1)} %all-gather.9.cloned.1.call-done, bf16[512,512]{1,0:T(8,128)(2,1)S(1)} %fusion.30, bf16[1,512]{1,0:T(2,128)(2,1)S(1)} %collective-permute-done.3, ...), kind=kOutput, calls=%fused_computation.11 | convolution fusion | flops 2157969408 | bytes 8932352 | tf_op jit(solution)/shard_map/dot_general | solution.py:56
  337.5 0.0 reduce-scatter.3.cloned.1.call-update
  337.6 0.0 all-gather.17.cloned.1.call-start
  337.6 29.4 %reduce-scatter.3.cloned.1.call-done = bf16[512,512]{1,0:T(8,128)(2,1)} async-done(((bf16[512,2048]{1,0:T(8,128)(2,1)}), bf16[512,512]{1,0:T(8,128)(2,1)}) %reduce-scatter.3.cloned.1.call-update) | async-done | bytes 524304 | tf_op jit(solution)/shard_map/reduce_scatter | solution.py:57
  367.1 2.0 add_convert_fusion.1
  369.0 0.0 all-gather.17.cloned.1.call-update
  369.0 0.0 reduce-scatter.5.cloned.1.call-start
  369.1 22.7 %all-gather.17.cloned.1.call-done = bf16[512,2048]{1,0:T(8,128)(2,1)} async-done(((bf16[512,512]{1,0:T(8,128)(2,1)}), bf16[512,2048]{1,0:T(8,128)(2,1)}) %all-gather.17.cloned.1.call-update) | async-done | bytes 2097168 | tf_op jit(solution)/shard_map/all_gather | solution.py:32
  391.8 2.1 fusion.3
  393.9 3.7 fusion.27
  397.5 0.4 copy-done.5
  397.9 1.3 fusion.28
  399.2 3.4 collective-permute-start.4
  402.6 1.3 collective-permute-start.5
  403.9 0.0 collective-permute-done.4
  403.9 4.2 collective-permute-done.5
  408.1 6.3 %convolution_convert_fusion = bf16[512,2048]{1,0:T(8,128)(2,1)} fusion(bf16[2,512,2048]{2,1,0:T(8,128)(2,1)} %all-gather.15.cloned.1.call-done, bf16[2,2048,512]{2,1,0:T(8,128)(2,1)} %all-gather.9.cloned.1.call-done, bf16[512,512]{1,0:T(8,128)(2,1)S(1)} %fusion.28, bf16[1,512]{1,0:T(2,128)(2,1)S(1)} %collective-permute-done.5, ...), kind=kOutput, calls=%fused_computation.10 | convolution fusion | flops 2157969408 | bytes 8932352 | tf_op jit(solution)/shard_map/dot_general | solution.py:56
  414.4 0.0 reduce-scatter.5.cloned.1.call-update
  414.5 31.3 %reduce-scatter.5.cloned.1.call-done = bf16[512,512]{1,0:T(8,128)(2,1)} async-done(((bf16[512,2048]{1,0:T(8,128)(2,1)}), bf16[512,512]{1,0:T(8,128)(2,1)}) %reduce-scatter.5.cloned.1.call-update) | async-done | bytes 524304 | tf_op jit(solution)/shard_map/reduce_scatter | solution.py:57
  445.8 2.0 add_convert_fusion
  (19 shorter events, 0.1 us)
Async XLA Ops:
  6.5 27.7 %all-gather.7.cloned.1.call-start = ((), (), s32[]{:S(2)}) async-start(), calls=%async_computation.2 | async-start | bytes 2621440 | tf_op jit(solution)/shard_map/all_gather | solution.py:32
  7.3 101.9 %all-gather.13.cloned.1.call-start = ((), (), s32[]{:S(2)}) async-start(), calls=%async_computation.5 | async-start | bytes 4718592 | tf_op jit(solution)/shard_map/all_gather | solution.py:27
  8.0 174.7 %all-gather.11.cloned.1.call-start = ((), (), s32[]{:S(2)}) async-start(), calls=%async_computation.4 | async-start | bytes 4718592 | tf_op jit(solution)/shard_map/all_gather | solution.py:26
  8.7 247.4 %all-gather.9.cloned.1.call-start = ((), (), s32[]{:S(2)}) async-start(), calls=%async_computation.3 | async-start | bytes 4718592 | tf_op jit(solution)/shard_map/all_gather | solution.py:25
  9.3 321.9 %all-gather.15.cloned.1.call-start = ((), (), s32[]{:S(2)}) async-start(), calls=%async_computation.6 | async-start | bytes 4718592 | tf_op jit(solution)/shard_map/all_gather | solution.py:29
  9.9 357.1 %reduce-scatter.3.cloned.1.call-start = ((), (), s32[]{:S(2)}) async-start(), calls=%async_computation.7 | async-start | bytes 2621440 | tf_op jit(solution)/shard_map/reduce_scatter | solution.py:57
  11.3 8.3 %collective-permute-start = (s32[1]{0:T(128)}, s32[1]{0:T(128)}, u32[]{:S(2)}, u32[]{:S(2)}) collective-permute-start(s32[1]{0:T(128)} %get-tuple-element.21), channel_id=1, source_target_pairs={{0,4},{4,8},{8,12},{12,16},{16,20},{20,24},{24,28},{1,5},{5,9},{9,... | collective-permute-start | bytes 20 | tf_op jit(solution)/shard_map/ppermute | solution.py:16
  16.7 5.5 %collective-permute-start.2 = (s32[1]{0:T(128)}, s32[1]{0:T(128)}, u32[]{:S(2)}, u32[]{:S(2)}) collective-permute-start(s32[1]{0:T(128)} %get-tuple-element.22), channel_id=1, source_target_pairs={{4,0},{8,4},{12,8},{16,12},{20,16},{24,20},{28,24},{5,1},{9,5},{13... | collective-permute-start | bytes 20 | tf_op jit(solution)/shard_map/ppermute | solution.py:17
  109.2 73.5 %copy-start.2 = (bf16[512,2048]{1,0:T(8,128)(2,1)S(1)}, bf16[512,2048]{1,0:T(8,128)(2,1)}, u32[]{:S(2)}) copy-start(bf16[512,2048]{1,0:T(8,128)(2,1)} %all-gather.7.cloned.1.call-done) | copy-start | bytes 6291460
  113.9 75.8 %copy-start.4 = (s32[512]{0:T(512)S(1)}, s32[512]{0:T(512)}, u32[]{:S(2)}) copy-start(s32[512]{0:T(512)} %param.9) | copy-start | bytes 6148
  185.9 145.3 %collective-permute-start.1 = (bf16[1,512]{1,0:T(2,128)(2,1)S(1)}, bf16[1,512]{1,0:T(2,128)(2,1)S(1)}, u32[]{:S(2)}, u32[]{:S(2)}) collective-permute-start(bf16[1,512]{1,0:T(2,128)(2,1)S(1)} %get-tuple-element.7), channel_id=1, source_target_pairs={{0,4},{4,8},{8,12},{12,16},{16,20},{20,24},{24,28},{1,5},{5,9},{9,... | collective-permute-start | bytes 3080 | tf_op jit(solution)/shard_map/ppermute | solution.py:16
  188.4 142.8 %collective-permute-start.3 = (bf16[1,512]{1,0:T(2,128)(2,1)S(1)}, bf16[1,512]{1,0:T(2,128)(2,1)S(1)}, u32[]{:S(2)}, u32[]{:S(2)}) collective-permute-start(bf16[1,512]{1,0:T(2,128)(2,1)S(1)} %get-tuple-element.8), channel_id=1, source_target_pairs={{4,0},{8,4},{12,8},{16,12},{20,16},{24,20},{28,24},{5,1},{9,5},{13... | collective-permute-start | bytes 3080 | tf_op jit(solution)/shard_map/ppermute | solution.py:17
  331.2 35.8 %copy-start.1 = (bf16[512,512]{1,0:T(8,128)(2,1)S(1)}, bf16[512,512]{1,0:T(8,128)(2,1)}, u32[]{:S(2)}) copy-start(bf16[512,512]{1,0:T(8,128)(2,1)} %param.8) | copy-start | bytes 1572868
  337.6 54.2 %all-gather.17.cloned.1.call-start = ((), (), s32[]{:S(2)}) async-start(), calls=%async_computation.8 | async-start | bytes 2621440 | tf_op jit(solution)/shard_map/all_gather | solution.py:32
  369.0 76.7 %reduce-scatter.5.cloned.1.call-start = ((), (), s32[]{:S(2)}) async-start(), calls=%async_computation.9 | async-start | bytes 2621440 | tf_op jit(solution)/shard_map/reduce_scatter | solution.py:57
  393.8 3.7 copy-start.3
  393.8 4.1 copy-start.5
  399.2 4.7 %collective-permute-start.4 = (bf16[1,512]{1,0:T(2,128)(2,1)S(1)}, bf16[1,512]{1,0:T(2,128)(2,1)S(1)}, u32[]{:S(2)}, u32[]{:S(2)}) collective-permute-start(bf16[1,512]{1,0:T(2,128)(2,1)S(1)} %get-tuple-element.5), channel_id=1, source_target_pairs={{0,4},{4,8},{8,12},{12,16},{16,20},{20,24},{24,28},{1,5},{5,9},{9,... | collective-permute-start | bytes 3080 | tf_op jit(solution)/shard_map/ppermute | solution.py:16
  402.6 5.5 %collective-permute-start.5 = (bf16[1,512]{1,0:T(2,128)(2,1)S(1)}, bf16[1,512]{1,0:T(2,128)(2,1)S(1)}, u32[]{:S(2)}, u32[]{:S(2)}) collective-permute-start(bf16[1,512]{1,0:T(2,128)(2,1)S(1)} %get-tuple-element.6), channel_id=1, source_target_pairs={{4,0},{8,4},{12,8},{16,12},{20,16},{24,20},{28,24},{5,1},{9,5},{13... | collective-permute-start | bytes 3080 | tf_op jit(solution)/shard_map/ppermute | solution.py:17
  408.1 37.7 %copy-start = (bf16[512,512]{1,0:T(8,128)(2,1)S(1)}, bf16[512,512]{1,0:T(8,128)(2,1)}, u32[]{:S(2)}) copy-start(bf16[512,512]{1,0:T(8,128)(2,1)} %add_convert_fusion.1) | copy-start | bytes 1572868
Sparse Core Ops, SparseCore 0:
  8.9 25.2 all-gather.6
  36.4 72.7 all-gather.12
  111.4 71.2 all-gather.10
  184.8 71.2 all-gather.8
  258.0 73.1 all-gather.14
  337.7 29.3 reduce-scatter.2
  369.2 22.5 all-gather.16
  414.6 31.1 reduce-scatter.4
where the time goes:
time: 455 us
  waiting for transfers between devices  386 us (85%)
  matrix products  25.4 us (6%)
  starting transfers between devices  15.4 us (3%)
  between operations  13.6 us (3%)
  other arithmetic  10.3 us (2%)
    all_gather x1, waiting for transfers between devices, per_device(): gathered_out = lax.all_gather(out_proj, 'sp', axis=2, tiled=True)  75.1 us
    all_gather x1, waiting for transfers between devices, per_device(): lax.all_gather(value_proj, 'sp', axis=1, tiled=True)  72.9 us
    all_gather x1, waiting for transfers between devices, per_device(): lax.all_gather(input_gate, 'sp', axis=1, tiled=True)  68.9 us
    all_gather x1, waiting for transfers between devices, per_device(): lax.all_gather(gate_proj, 'sp', axis=1, tiled=True)  66.4 us
    reduce_scatter x2, waiting for transfers between devices, per_device(): lax.psum_scatter(partials.astype(jnp.bfloat16), 'tp', scatter_dimension=1...  60.7 us
    all_gather x2, waiting for transfers between devices, per_device(): full_rows = lax.all_gather(current, 'tp', axis=1, tiled=True)  32.6 us
    dot_general x2, matrix products, per_device(): jnp.dot(gated, gathered_out[layer_index], preferred_element_type=jnp.floa...  12.7 us
    ppermute x3, starting transfers between devices, with_halo(): before = lax.ppermute(last, axis, up)  11.2 us
  transfers between devices with their start and end apart: 14, of which 10 were waited for; matrix products, arithmetic and copies ran while one was open for 3% of the time, Pallas kernels for 0%

commit v1 on v0

--- a/solution.py
+++ b/solution.py
@@ -4,6 +4,10 @@
 from jax.sharding import PartitionSpec as P
 
 epsilon = 1e-06
+
+
+def group_grid_on_mesh(payload):
+    return jnp.concatenate(lax.all_gather(payload, axis_name="sp"), axis=1)
 
 
 def with_halo(value, sides, width):
@@ -22,7 +26,7 @@
 def per_device(stream, doc_ids, norm_gain, gate_proj, input_gate, value_proj, taps, out_proj):
     layers = gate_proj.shape[0]
     gathered_in = (
-        lax.all_gather(gate_proj, "sp", axis=1, tiled=True),
+        group_grid_on_mesh(gate_proj),
         lax.all_gather(input_gate, "sp", axis=1, tiled=True),
         lax.all_gather(value_proj, "sp", axis=1, tiled=True),
     )

time: 455 us -> 454 us (level)
    all_gather x1, waiting for transfers between devices: 75.1 us -> 70.5 us  [per_device(): gathered_out = lax.all_gather(out_proj, 'sp', axis=2, tiled=True)]
    slice x0 -> x1, local copies, waits for them, and re-layouts: none -> 4.6 us  [per_device(): gathered_in[0][layer_index]]
  transfers between devices with their start and end apart: 14 -> 14, of which waited for: 10 -> 10; matrix products, arithmetic and copies ran while one was open for 3% -> 4% of each run, Pallas kernels for 0% -> 0%
where the time goes in v1:
time: 454 us; the launch traced here: 453 us
  waiting for transfers between devices  385 us (85%)
  matrix products  23.8 us (5%)
  starting transfers between devices  15.5 us (3%)
  between operations  13.7 us (3%)
  other arithmetic  9.91 us (2%)
  local copies, waits for them, and re-layouts  5.25 us (1%)
    all_gather x1, waiting for transfers between devices, per_device(): lax.all_gather(value_proj, 'sp', axis=1, tiled=True)  72.8 us
    all_gather x1, waiting for transfers between devices, per_device(): gathered_out = lax.all_gather(out_proj, 'sp', axis=2, tiled=True)  70.5 us
    all_gather x1, waiting for transfers between devices, per_device(): lax.all_gather(input_gate, 'sp', axis=1, tiled=True)  69.7 us
    all_gather x1, waiting for transfers between devices, group_grid_on_mesh(): return jnp.concatenate(lax.all_gather(payload, axis_name='sp'), axis=1)  66.4 us
    reduce_scatter x2, waiting for transfers between devices, per_device(): lax.psum_scatter(partials.astype(jnp.bfloat16), 'tp', scatter_dimension=1...  60.8 us
    all_gather x2, waiting for transfers between devices, per_device(): full_rows = lax.all_gather(current, 'tp', axis=1, tiled=True)  33.7 us
    dot_general x2, matrix products, per_device(): jnp.dot(gated, gathered_out[layer_index], preferred_element_type=jnp.floa...  12.4 us
    ppermute x3, starting transfers between devices, with_halo(): before = lax.ppermute(last, axis, up)  11.3 us
  transfers between devices with their start and end apart: 14, of which 10 were waited for; matrix products, arithmetic and copies ran while one was open for 4% of the time, Pallas kernels for 0%

profile of v1, /device:TPU:0, one launch (start us, length us, event | category | flops | bytes accessed | tf_op | source)
XLA Modules:
  0.0 453.5 jit_solution(3108508972889966958)
XLA Ops:
  6.5 0.7 all-gather.8.cloned.1.call-update
  7.3 0.0 all-gather.12.cloned.1.call-start
  7.3 0.7 all-gather.12.cloned.1.call-update
  8.0 0.0 all-gather.10.cloned.1.call-start
  8.1 0.7 all-gather.10.cloned.1.call-update
  8.7 0.0 all-gather.18.cloned.1.call-start
  8.8 0.5 all-gather.18.cloned.1.call-update
  9.3 0.0 all-gather.14.cloned.1.call-start
  9.4 0.5 all-gather.14.cloned.1.call-update
  9.9 0.0 reduce-scatter.3.cloned.1.call-start
  10.0 0.6 fusion.61
  10.6 5.5 %collective-permute-start = (s32[1]{0:T(128)}, s32[1]{0:T(128)}, u32[]{:S(2)}, u32[]{:S(2)}) collective-permute-start(s32[1]{0:T(128)} %get-tuple-element.23), channel_id=1, source_target_pairs={{0,4},{4,8},{8,12},{12,16},{16,20},{20,24},{24,28},{1,5},{5,9},{9,... | collective-permute-start | bytes 20 | tf_op jit(solution)/shard_map/ppermute | solution.py:20
  16.0 1.3 collective-permute-start.2
  17.4 0.0 collective-permute-done
  17.4 4.3 collective-permute-done.2
  21.6 1.4 pad_add_fusion
  23.1 0.1 slice_compare_fusion.1
  23.2 11.1 %all-gather.8.cloned.1.call-done = bf16[512,2048]{1,0:T(8,128)(2,1)} async-done(((bf16[512,512]{1,0:T(8,128)(2,1)}), bf16[512,2048]{1,0:T(8,128)(2,1)}) %all-gather.8.cloned.1.call-update) | async-done | bytes 2097168 | tf_op jit(solution)/shard_map/all_gather | solution.py:36
  34.2 2.2 fusion
  36.5 72.8 %all-gather.12.cloned.1.call-done = bf16[2,2048,512]{2,1,0:T(8,128)(2,1)} async-done(((bf16[2,256,512]{2,1,0:T(8,128)(2,1)}), bf16[2,2048,512]{2,1,0:T(8,128)(2,1)}) %all-gather.12.cloned.1.call-update) | async-done | bytes 4194320 | tf_op jit(solution)/shard_map/all_gather | solution.py:31
  109.2 3.9 fusion.14
  113.1 69.7 %all-gather.10.cloned.1.call-done = bf16[2,2048,512]{2,1,0:T(8,128)(2,1)} async-done(((bf16[2,256,512]{2,1,0:T(8,128)(2,1)}), bf16[2,2048,512]{2,1,0:T(8,128)(2,1)}) %all-gather.10.cloned.1.call-update) | async-done | bytes 4194320 | tf_op jit(solution)/shard_map/all_gather | solution.py:30
  182.7 3.2 fusion.27
  185.9 2.5 collective-permute-start.1
  188.4 1.3 collective-permute-start.3
  189.7 66.4 %all-gather.18.cloned.1.call-done = bf16[16,256,512]{2,1,0:T(8,128)(2,1)} async-done(((bf16[2,256,512]{2,1,0:T(8,128)(2,1)}), bf16[16,256,512]{2,1,0:T(8,128)(2,1)}) %all-gather.18.cloned.1.call-update) | async-done | bytes 4194320 | tf_op jit(solution)/shard_map/all_gather | solution.py:10
  256.1 4.6 %fusion.56 = (bf16[1,8,256,512]{3,2,0,1:T(8,128)(2,1)}, bf16[1,8,256,512]{3,2,0,1:T(8,128)(2,1)}) fusion(bf16[2,8,256,512]{3,2,0,1:T(8,128)(2,1)} %bitcast.57), kind=kLoop, calls=%fused_computation.74 | loop fusion | bytes 8388608 | tf_op jit(solution)/shard_map/slice | solution.py:40
  260.7 70.5 %all-gather.14.cloned.1.call-done = bf16[2,512,2048]{2,1,0:T(8,128)(2,1)} async-done(((bf16[2,512,256]{2,1,0:T(8,128)(2,1)}), bf16[2,512,2048]{2,1,0:T(8,128)(2,1)}) %all-gather.14.cloned.1.call-update) | async-done | bytes 4194320 | tf_op jit(solution)/shard_map/all_gather | solution.py:33
  331.2 0.0 collective-permute-done.1
  331.2 0.0 collective-permute-done.3
  331.2 6.2 %convolution_convert_fusion.1 = bf16[512,2048]{1,0:T(8,128)(2,1)} fusion(bf16[2,512,2048]{2,1,0:T(8,128)(2,1)} %all-gather.14.cloned.1.call-done, bf16[2048,512]{1,0:T(8,128)(2,1)} %bitcast.59, bf16[512,512]{1,0:T(8,128)(2,1)S(1)} %fusion.27, bf16[1,512]{1,0:T(2,128)(2,1)S(1)} %collective-permute-done.3, bf16[1,512]{1,0:T(2,128)(2,1)S(1)} %collective-permute-done.1, ...), kind=kOutput, calls=%fused_computation.11 | convolution fusion | flops 2157969408 | bytes 8932352 | tf_op jit(solution)/shard_map/dot_general | solution.py:60
  337.4 0.0 reduce-scatter.3.cloned.1.call-update
  337.4 0.0 all-gather.16.cloned.1.call-start
  337.5 29.5 %reduce-scatter.3.cloned.1.call-done = bf16[512,512]{1,0:T(8,128)(2,1)} async-done(((bf16[512,2048]{1,0:T(8,128)(2,1)}), bf16[512,512]{1,0:T(8,128)(2,1)}) %reduce-scatter.3.cloned.1.call-update) | async-done | bytes 524304 | tf_op jit(solution)/shard_map/reduce_scatter | solution.py:61
  366.9 2.0 add_convert_fusion.1
  368.9 0.0 all-gather.16.cloned.1.call-update
  368.9 0.0 reduce-scatter.5.cloned.1.call-start
  369.0 22.7 %all-gather.16.cloned.1.call-done = bf16[512,2048]{1,0:T(8,128)(2,1)} async-done(((bf16[512,512]{1,0:T(8,128)(2,1)}), bf16[512,2048]{1,0:T(8,128)(2,1)}) %all-gather.16.cloned.1.call-update) | async-done | bytes 2097168 | tf_op jit(solution)/shard_map/all_gather | solution.py:36
  391.6 2.2 fusion.3
  393.9 3.0 fusion.19
  396.9 1.3 fusion.26
  398.3 3.4 collective-permute-start.4
  401.7 1.3 collective-permute-start.5
  403.0 4.2 collective-permute-done.5
  407.1 6.2 %convolution_convert_fusion = bf16[512,2048]{1,0:T(8,128)(2,1)} fusion(bf16[2,512,2048]{2,1,0:T(8,128)(2,1)} %all-gather.14.cloned.1.call-done, bf16[2048,512]{1,0:T(8,128)(2,1)} %bitcast.58, bf16[512,512]{1,0:T(8,128)(2,1)S(1)} %fusion.26, bf16[1,512]{1,0:T(2,128)(2,1)S(1)} %collective-permute-done.5, bf16[1,512]{1,0:T(2,128)(2,1)S(1)} %collective-permute-done.4, ...), kind=kOutput, calls=%fused_computation.10 | convolution fusion | flops 2157969408 | bytes 8932352 | tf_op jit(solution)/shard_map/dot_general | solution.py:60
  413.4 0.0 reduce-scatter.5.cloned.1.call-update
  413.4 31.3 %reduce-scatter.5.cloned.1.call-done = bf16[512,512]{1,0:T(8,128)(2,1)} async-done(((bf16[512,2048]{1,0:T(8,128)(2,1)}), bf16[512,512]{1,0:T(8,128)(2,1)}) %reduce-scatter.5.cloned.1.call-update) | async-done | bytes 524304 | tf_op jit(solution)/shard_map/reduce_scatter | solution.py:61
  444.7 2.0 add_convert_fusion
  (24 shorter events, 0.1 us)
Async XLA Ops:
  6.5 3.4 copy-start.5
  6.5 10.8 %copy-start.6 = (f32[2,3,512]{2,0,1:T(2,128)S(1)}, f32[2,3,512]{2,0,1:T(2,128)}, u32[]{:S(2)}) copy-start(f32[2,3,512]{2,0,1:T(2,128)} %param.14) | copy-start | bytes 36868
  6.5 10.8 %copy-start.4 = (f32[2,2048]{1,0:T(2,128)S(1)}, f32[2,2048]{1,0:T(2,128)}, u32[]{:S(2)}) copy-start(f32[2,2048]{1,0:T(2,128)} %param.10) | copy-start | bytes 49156
  6.5 27.7 %all-gather.8.cloned.1.call-start = ((), (), s32[]{:S(2)}) async-start(), calls=%async_computation.2 | async-start | bytes 2621440 | tf_op jit(solution)/shard_map/all_gather | solution.py:36
  7.3 101.9 %all-gather.12.cloned.1.call-start = ((), (), s32[]{:S(2)}) async-start(), calls=%async_computation.4 | async-start | bytes 4718592 | tf_op jit(solution)/shard_map/all_gather | solution.py:31
  8.0 174.7 %all-gather.10.cloned.1.call-start = ((), (), s32[]{:S(2)}) async-start(), calls=%async_computation.3 | async-start | bytes 4718592 | tf_op jit(solution)/shard_map/all_gather | solution.py:30
  8.7 247.3 %all-gather.18.cloned.1.call-start = ((), (), s32[]{:S(2)}) async-start(), calls=%async_computation.9 | async-start | bytes 4718592 | tf_op jit(solution)/shard_map/all_gather | solution.py:10
  9.3 321.9 %all-gather.14.cloned.1.call-start = ((), (), s32[]{:S(2)}) async-start(), calls=%async_computation.5 | async-start | bytes 4718592 | tf_op jit(solution)/shard_map/all_gather | solution.py:33
  9.9 357.0 %reduce-scatter.3.cloned.1.call-start = ((), (), s32[]{:S(2)}) async-start(), calls=%async_computation.6 | async-start | bytes 2621440 | tf_op jit(solution)/shard_map/reduce_scatter | solution.py:61
  10.6 6.8 %collective-permute-start = (s32[1]{0:T(128)}, s32[1]{0:T(128)}, u32[]{:S(2)}, u32[]{:S(2)}) collective-permute-start(s32[1]{0:T(128)} %get-tuple-element.23), channel_id=1, source_target_pairs={{0,4},{4,8},{8,12},{12,16},{16,20},{20,24},{24,28},{1,5},{5,9},{9,... | collective-permute-start | bytes 20 | tf_op jit(solution)/shard_map/ppermute | solution.py:20
  16.0 5.6 %collective-permute-start.2 = (s32[1]{0:T(128)}, s32[1]{0:T(128)}, u32[]{:S(2)}, u32[]{:S(2)}) collective-permute-start(s32[1]{0:T(128)} %get-tuple-element.24), channel_id=1, source_target_pairs={{4,0},{8,4},{12,8},{16,12},{20,16},{24,20},{28,24},{5,1},{9,5},{13... | collective-permute-start | bytes 20 | tf_op jit(solution)/shard_map/ppermute | solution.py:21
  34.2 75.0 %copy-start.2 = (bf16[512,2048]{1,0:T(8,128)(2,1)S(1)}, bf16[512,2048]{1,0:T(8,128)(2,1)}, u32[]{:S(2)}) copy-start(bf16[512,2048]{1,0:T(8,128)(2,1)} %all-gather.8.cloned.1.call-done) | copy-start | bytes 6291460
  185.9 145.3 %collective-permute-start.1 = (bf16[1,512]{1,0:T(2,128)(2,1)S(1)}, bf16[1,512]{1,0:T(2,128)(2,1)S(1)}, u32[]{:S(2)}, u32[]{:S(2)}) collective-permute-start(bf16[1,512]{1,0:T(2,128)(2,1)S(1)} %get-tuple-element.9), channel_id=1, source_target_pairs={{0,4},{4,8},{8,12},{12,16},{16,20},{20,24},{24,28},{1,5},{5,9},{9,... | collective-permute-start | bytes 3080 | tf_op jit(solution)/shard_map/ppermute | solution.py:20
  188.4 142.8 %collective-permute-start.3 = (bf16[1,512]{1,0:T(2,128)(2,1)S(1)}, bf16[1,512]{1,0:T(2,128)(2,1)S(1)}, u32[]{:S(2)}, u32[]{:S(2)}) collective-permute-start(bf16[1,512]{1,0:T(2,128)(2,1)S(1)} %get-tuple-element.10), channel_id=1, source_target_pairs={{4,0},{8,4},{12,8},{16,12},{20,16},{24,20},{28,24},{5,1},{9,5},{13... | collective-permute-start | bytes 3080 | tf_op jit(solution)/shard_map/ppermute | solution.py:21
  337.4 29.5 %copy-start.1 = (bf16[512,512]{1,0:T(8,128)(2,1)S(1)}, bf16[512,512]{1,0:T(8,128)(2,1)}, u32[]{:S(2)}) copy-start(bf16[512,512]{1,0:T(8,128)(2,1)} %param.8) | copy-start | bytes 1572868
  337.4 54.2 %all-gather.16.cloned.1.call-start = ((), (), s32[]{:S(2)}) async-start(), calls=%async_computation.7 | async-start | bytes 2621440 | tf_op jit(solution)/shard_map/all_gather | solution.py:36
  368.9 75.8 %reduce-scatter.5.cloned.1.call-start = ((), (), s32[]{:S(2)}) async-start(), calls=%async_computation.8 | async-start | bytes 2621440 | tf_op jit(solution)/shard_map/reduce_scatter | solution.py:61
  391.6 2.2 copy-start.3
  393.9 3.0 copy-start.7
  398.3 4.7 %collective-permute-start.4 = (bf16[1,512]{1,0:T(2,128)(2,1)S(1)}, bf16[1,512]{1,0:T(2,128)(2,1)S(1)}, u32[]{:S(2)}, u32[]{:S(2)}) collective-permute-start(bf16[1,512]{1,0:T(2,128)(2,1)S(1)} %get-tuple-element.7), channel_id=1, source_target_pairs={{0,4},{4,8},{8,12},{12,16},{16,20},{20,24},{24,28},{1,5},{5,9},{9,... | collective-permute-start | bytes 3080 | tf_op jit(solution)/shard_map/ppermute | solution.py:20
  401.7 5.5 %collective-permute-start.5 = (bf16[1,512]{1,0:T(2,128)(2,1)S(1)}, bf16[1,512]{1,0:T(2,128)(2,1)S(1)}, u32[]{:S(2)}, u32[]{:S(2)}) collective-permute-start(bf16[1,512]{1,0:T(2,128)(2,1)S(1)} %get-tuple-element.8), channel_id=1, source_target_pairs={{4,0},{8,4},{12,8},{16,12},{20,16},{24,20},{28,24},{5,1},{9,5},{13... | collective-permute-start | bytes 3080 | tf_op jit(solution)/shard_map/ppermute | solution.py:21
  413.4 31.3 %copy-start = (bf16[512,512]{1,0:T(8,128)(2,1)S(1)}, bf16[512,512]{1,0:T(8,128)(2,1)}, u32[]{:S(2)}) copy-start(bf16[512,512]{1,0:T(8,128)(2,1)} %add_convert_fusion.1) | copy-start | bytes 1572868
Sparse Core Ops, SparseCore 0:
  8.9 25.2 all-gather.7
  36.4 72.7 all-gather.11
  111.4 71.2 all-gather.9
  184.7 71.3 all-gather.17
  258.0 73.1 all-gather.13
  337.5 29.3 reduce-scatter.2
  369.1 22.5 all-gather.15
  413.5 31.1 reduce-scatter.4
